TPU v7x, 32 devices: a whole 2x2x4 slice. The times are simulated.
32 devices in a mesh: kv: 16 (over z, y, x), tp: 2 (over core).
Axes of the slice: x: 2, y: 2, z: 4, core: 2. Of those that a mesh axis runs over, the one named last changes fastest.
Arguments:
- tokens: bfloat16 [64, 4, 2048], P('kv', None, 'tp'), may hold values from -6 to 6
- input_gain: float32 [2048], replicated, may hold values from 0.1 to 1.9
- gate_weight: bfloat16 [2048, 4096], P('kv', 'tp'), may hold values from -0.125 to 0.125
- value_weight: bfloat16 [2048, 4096], P('kv', 'tp'), may hold values from -0.125 to 0.125
- write_weight: bfloat16 [2048, 1024], P('kv', 'tp'), may hold values from -0.125 to 0.125
- read_weight: bfloat16 [2048, 1024], P('kv', 'tp'), may hold values from -0.125 to 0.125
- step_weight: bfloat16 [2048, 64], replicated, may hold values from -0.125 to 0.125
- conv_value: float32 [4, 4096], P(None, 'tp'), may hold values from -3 to 3
- conv_write: float32 [4, 1024], P(None, 'tp'), may hold values from -3 to 3
- conv_read: float32 [4, 1024], P(None, 'tp'), may hold values from -3 to 3
- step_bias: float32 [64], P('tp'), may hold values from -4 to -1
- decay_log: float32 [64], P('tp'), may hold values from 0 to 2.8
- skip_gain: float32 [64], P('tp'), may hold values from 0.5 to 1.5
- output_gain: float32 [4096], P('tp'), may hold values from 0.1 to 1.9
- out_weight: bfloat16 [4096, 2048], P('tp', 'kv'), may hold values from -0.09375 to 0.09375
- base_state: float32 [64, 64, 64, 128], P('kv', 'tp'), may hold values from -2 to 2
- past_value: bfloat16 [64, 7, 4096], P('kv', None, 'tp'), may hold values from -6 to 6
- past_write: bfloat16 [64, 7, 1024], P('kv', None, 'tp'), may hold values from -6 to 6
- past_read: bfloat16 [64, 7, 1024], P('kv', None, 'tp'), may hold values from -6 to 6
- past_step: bfloat16 [64, 4, 64], P('kv', None, 'tp'), may hold values from -4 to 4
- accepted: int32 [64], P('kv'), may hold values from 1 to 4
Outputs:
- mixed: bfloat16 [64, 4, 2048], P('kv', None, 'tp')
- root_state: float32 [64, 64, 64, 128], P('kv', 'tp')
- next_value: bfloat16 [64, 7, 4096], P('kv', None, 'tp')
- next_write: bfloat16 [64, 7, 1024], P('kv', None, 'tp')
- next_read: bfloat16 [64, 7, 1024], P('kv', None, 'tp')
- next_step: bfloat16 [64, 4, 64], P('kv', None, 'tp')
Inputs may be any that keep to these rules, and one draw needn't show every extreme that they name: Every entry of `accepted` is an integer from 1 to 4 (at least one of the last step's proposals is always accepted).
All inputs are finite; a program needn't handle non-finite values.
Results may differ from a plain program's by a relative error of at most 0.018.
Values may be sent and summed in bfloat16 or wider, within the bound.
No kernel may reach another device: no remote copies, remote signals or barrier semaphores. Data moves between devices by JAX's collectives and lax.ppermute only.
A program may use at most 64 MiB of HBM per device.

v0:
```python
import jax
import jax.numpy as jnp
from jax import lax
from jax.sharding import PartitionSpec as P

STATE_DIM = 128
CONV_W = 4
EPSILON = 1e-06


def causal_conv(rows, kernel):
    width = kernel.shape[0]
    count = rows.shape[0] - width + 1
    total = kernel[0] * rows[0:count]
    for offset in range(1, width):
        total = total + kernel[offset] * rows[offset : offset + count]
    return total


def advance(
    past_x,
    past_b,
    past_c,
    past_dt,
    taken,
    state_zero,
    value_now,
    write_now,
    read_now,
    gate_now,
    step_now,
    conv_value,
    conv_write,
    conv_read,
    step_bias,
    decay_log,
    skip_gain,
    output_gain,
):
    highest = lax.Precision.HIGHEST
    proposals = value_now.shape[0]
    head_count = step_bias.shape[0]
    group_count = write_now.shape[1] // STATE_DIM
    per_group = head_count // group_count
    head_width = value_now.shape[1] // head_count
    rate = jnp.exp(decay_log)
    prev_x = jax.nn.silu(causal_conv(past_x.astype(jnp.float32), conv_value)).reshape(
        proposals, head_count, head_width
    )
    prev_b = jax.nn.silu(causal_conv(past_b.astype(jnp.float32), conv_write)).reshape(
        proposals, group_count, STATE_DIM
    )
    prev_b = jnp.repeat(prev_b, per_group, axis=1)
    prev_dt = jax.nn.softplus(past_dt.astype(jnp.float32) + step_bias)
    live = (jnp.arange(proposals, dtype=jnp.int32) < taken)[:, None]
    prev_log = jnp.where(live, -rate * prev_dt, jnp.zeros_like(prev_dt))
    total_log = jnp.sum(prev_log, axis=0)
    tail_log = total_log - jnp.cumsum(prev_log, axis=0)
    weight_now = jnp.where(live, jnp.exp(tail_log) * prev_dt, jnp.zeros_like(prev_dt))
    root = jnp.exp(total_log)[:, None, None] * state_zero + jnp.einsum(
        "sh,shp,shn->hpn", weight_now, prev_x, prev_b, precision=highest
    )
    window_x = jnp.concatenate(
        [lax.dynamic_slice_in_dim(past_x, taken, CONV_W - 1, 0), value_now], axis=0
    )
    window_b = jnp.concatenate(
        [lax.dynamic_slice_in_dim(past_b, taken, CONV_W - 1, 0), write_now], axis=0
    )
    window_c = jnp.concatenate(
        [lax.dynamic_slice_in_dim(past_c, taken, CONV_W - 1, 0), read_now], axis=0
    )
    cur_x = jax.nn.silu(causal_conv(window_x.astype(jnp.float32), conv_value)).reshape(
        proposals, head_count, head_width
    )
    cur_b = jax.nn.silu(causal_conv(window_b.astype(jnp.float32), conv_write)).reshape(
        proposals, group_count, STATE_DIM
    )
    cur_c = jax.nn.silu(causal_conv(window_c.astype(jnp.float32), conv_read)).reshape(
        proposals, group_count, STATE_DIM
    )
    cur_b = jnp.repeat(cur_b, per_group, axis=1)
    cur_c = jnp.repeat(cur_c, per_group, axis=1)
    cur_dt = jax.nn.softplus(step_now.astype(jnp.float32) + step_bias)
    logs = jnp.cumsum(-rate * cur_dt, axis=0)
    carried = jnp.einsum("thn,hpn->thp", cur_c, root, precision=highest) * jnp.exp(logs)[:, :, None]
    lower = (jnp.arange(proposals)[:, None] >= jnp.arange(proposals)[None, :])[:, :, None]
    diff = logs[:, None, :] - logs[None, :, :]
    decay = jnp.where(
        lower, jnp.exp(jnp.where(lower, diff, jnp.zeros_like(diff))), jnp.zeros_like(diff)
    )
    scores = (
        jnp.einsum("thn,shn->tsh", cur_c, cur_b, precision=highest) * decay * cur_dt[None, :, :]
    )
    inner = jnp.einsum("tsh,shp->thp", scores, cur_x, precision=highest)
    mixed = carried + inner + skip_gain[None, :, None] * cur_x
    gated = mixed.reshape(proposals, -1) * jax.nn.silu(gate_now.astype(jnp.float32))
    grouped = gated.reshape(proposals, group_count, -1)
    grouped = grouped * lax.rsqrt(jnp.mean(grouped * grouped, axis=-1, keepdims=True) + EPSILON)
    result = (grouped.reshape(proposals, -1) * output_gain).astype(jnp.bfloat16)
    return (result, root, window_x, window_b, window_c)


def on_device(
    tokens,
    input_gain,
    gate_weight,
    value_weight,
    write_weight,
    read_weight,
    step_weight,
    conv_value,
    conv_write,
    conv_read,
    step_bias,
    decay_log,
    skip_gain,
    output_gain,
    out_weight,
    base_state,
    past_value,
    past_write,
    past_read,
    past_step,
    accepted,
):
    whole = lax.all_gather(tokens, "tp", axis=2, tiled=True)
    seq_local, proposals, width = whole.shape
    rows = whole.astype(jnp.float32)
    normed = (
        rows * lax.rsqrt(jnp.mean(rows * rows, axis=-1, keepdims=True) + EPSILON) * input_gain
    ).astype(jnp.bfloat16)
    flat = normed.reshape(seq_local * proposals, width)
    token_count = flat.shape[0]
    head_count = step_bias.shape[0]
    own_step = lax.dynamic_slice_in_dim(
        step_weight, lax.axis_index("tp") * head_count, head_count, 1
    )
    step_now = jnp.dot(flat, own_step, preferred_element_type=jnp.float32).astype(jnp.bfloat16)
    slabs = (
        lax.all_to_all(gate_weight, "kv", split_axis=1, concat_axis=0, tiled=True),
        lax.all_to_all(value_weight, "kv", split_axis=1, concat_axis=0, tiled=True),
        lax.all_to_all(write_weight, "kv", split_axis=1, concat_axis=0, tiled=True),
        lax.all_to_all(read_weight, "kv", split_axis=1, concat_axis=0, tiled=True),
    )
    spans = [slab.shape[1] for slab in slabs]
    narrow = jnp.concatenate(slabs, axis=1)
    everyone = jnp.dot(
        lax.all_gather(flat, "kv", axis=0, tiled=True), narrow, preferred_element_type=jnp.float32
    ).astype(jnp.bfloat16)
    returned = lax.all_to_all(everyone, "kv", split_axis=0, concat_axis=1, tiled=True)
    ranks = lax.axis_size("kv")
    returned = returned.reshape(token_count, ranks, sum(spans))
    pieces_out = []
    offset = 0
    for span in spans:
        pieces_out.append(returned[:, :, offset : offset + span].reshape(token_count, ranks * span))
        offset = offset + span
    gate_now, value_now, write_now, read_now = pieces_out
    shaped = [
        item.reshape(seq_local, proposals, item.shape[1])
        for item in (value_now, write_now, read_now, gate_now, step_now)
    ]
    stepper = jax.vmap(advance, in_axes=(0,) * 11 + (None,) * 7)
    normal_out, root_state, next_value, next_write, next_read = stepper(
        past_value,
        past_write,
        past_read,
        past_step,
        accepted,
        base_state,
        shaped[0],
        shaped[1],
        shaped[2],
        shaped[3],
        shaped[4],
        conv_value,
        conv_write,
        conv_read,
        step_bias,
        decay_log,
        skip_gain,
        output_gain,
    )
    flat_y = normal_out.reshape(token_count, -1)
    partial_sum = jnp.dot(
        flat_y,
        lax.all_gather(out_weight, "kv", axis=1, tiled=True),
        preferred_element_type=jnp.float32,
    )
    summed = lax.psum_scatter(
        partial_sum.astype(jnp.bfloat16), "tp", scatter_dimension=1, tiled=True
    ).astype(jnp.float32)
    mixed = summed.astype(jnp.bfloat16).reshape(seq_local, proposals, summed.shape[1])
    return (mixed, root_state, next_value, next_write, next_read, shaped[4])


def solution(mesh):
    return jax.shard_map(
        on_device,
        mesh=mesh,
        in_specs=(
            P("kv", None, "tp"),
            P(),
            P("kv", "tp"),
            P("kv", "tp"),
            P("kv", "tp"),
            P("kv", "tp"),
            P(),
            P(None, "tp"),
            P(None, "tp"),
            P(None, "tp"),
            P("tp"),
            P("tp"),
            P("tp"),
            P("tp"),
            P("tp", "kv"),
            P("kv", "tp", None, None),
            P("kv", None, "tp"),
            P("kv", None, "tp"),
            P("kv", None, "tp"),
            P("kv", None, "tp"),
            P("kv"),
        ),
        out_specs=(
            P("kv", None, "tp"),
            P("kv", "tp", None, None),
            P("kv", None, "tp"),
            P("kv", None, "tp"),
            P("kv", None, "tp"),
            P("kv", None, "tp"),
        ),
        check_vma=False,
    )
```

profile of v0, /device:TPU:0, one launch (start us, length us, event | category | flops | bytes accessed | tf_op | source)
XLA Modules:
  0.0 240.1 jit_solution(14722465819496785952)
XLA Ops:
  7.3 2.3 all_gather.9
  12.0 1.7 copy.196
  13.7 8.2 %all-to-all-start.2 = ((bf16[128,16,32]{0,2,1:T(8,128)(2,1)}), bf16[128,16,32]{0,2,1:T(8,128)(2,1)S(1)}, u32[]{:S(2)}, u32[]{:S(2)}) async-start(bf16[128,16,32]{0,2,1:T(8,128)(2,1)} %bitcast.19), calls=%async_computation.2 | async-start | bytes 262144 | tf_op jit(solution)/shard_map/all_to_all | solution.py:142
  21.9 1.7 copy.198
  23.6 6.5 %all-to-all-done.2 = bf16[128,16,32]{0,2,1:T(8,128)(2,1)S(1)} async-done(((bf16[128,16,32]{0,2,1:T(8,128)(2,1)}), bf16[128,16,32]{0,2,1:T(8,128)(2,1)S(1)}, u32[]{:S(2)}, u32[]{:S(2)}) %all-to-all-start.2) | async-done | bytes 131104 | tf_op jit(solution)/shard_map/all_to_all | solution.py:142
  30.1 3.5 %all-to-all-start.3 = ((bf16[128,16,32]{0,2,1:T(8,128)(2,1)}), bf16[128,16,32]{0,2,1:T(8,128)(2,1)S(1)}, u32[]{:S(2)}, u32[]{:S(2)}) async-start(bf16[128,16,32]{0,2,1:T(8,128)(2,1)} %bitcast.22), calls=%async_computation.3 | async-start | bytes 262144 | tf_op jit(solution)/shard_map/all_to_all | solution.py:143
  33.6 2.0 copy.192
  35.6 5.7 %all-to-all-done.3 = bf16[128,16,32]{0,2,1:T(8,128)(2,1)S(1)} async-done(((bf16[128,16,32]{0,2,1:T(8,128)(2,1)}), bf16[128,16,32]{0,2,1:T(8,128)(2,1)S(1)}, u32[]{:S(2)}, u32[]{:S(2)}) %all-to-all-start.3) | async-done | bytes 131104 | tf_op jit(solution)/shard_map/all_to_all | solution.py:143
  41.4 3.6 %all-to-all-start = ((bf16[128,16,128]{0,2,1:T(8,128)(2,1)}), bf16[128,16,128]{0,2,1:T(8,128)(2,1)S(1)}, u32[]{:S(2)}, u32[]{:S(2)}) async-start(bf16[128,16,128]{0,2,1:T(8,128)(2,1)} %bitcast.13), calls=%async_computation | async-start | bytes 1048576 | tf_op jit(solution)/shard_map/all_to_all | solution.py:140
  46.3 13.3 %all-to-all-done = bf16[128,16,128]{0,2,1:T(8,128)(2,1)S(1)} async-done(((bf16[128,16,128]{0,2,1:T(8,128)(2,1)}), bf16[128,16,128]{0,2,1:T(8,128)(2,1)S(1)}, u32[]{:S(2)}, u32[]{:S(2)}) %all-to-all-start) | async-done | bytes 524320 | tf_op jit(solution)/shard_map/all_to_all | solution.py:140
  59.6 3.9 %all-to-all-start.1 = ((bf16[128,16,128]{0,2,1:T(8,128)(2,1)}), bf16[128,16,128]{0,2,1:T(8,128)(2,1)S(1)}, u32[]{:S(2)}, u32[]{:S(2)}) async-start(bf16[128,16,128]{0,2,1:T(8,128)(2,1)} %bitcast.16), calls=%async_computation.1 | async-start | bytes 1048576 | tf_op jit(solution)/shard_map/all_to_all | solution.py:141
  67.2 12.8 %all-to-all-done.1 = bf16[128,16,128]{0,2,1:T(8,128)(2,1)S(1)} async-done(((bf16[128,16,128]{0,2,1:T(8,128)(2,1)}), bf16[128,16,128]{0,2,1:T(8,128)(2,1)S(1)}, u32[]{:S(2)}, u32[]{:S(2)}) %all-to-all-start.1) | async-done | bytes 524320 | tf_op jit(solution)/shard_map/all_to_all | solution.py:141
  80.3 2.3 fusion.10
  83.5 4.8 %all-to-all-start.4 = ((bf16[16,16,320]{2,1,0:T(8,128)(2,1)}), bf16[16,16,320]{2,1,0:T(8,128)(2,1)S(1)}, u32[]{:S(2)}, u32[]{:S(2)}) async-start(bf16[16,16,320]{2,1,0:T(8,128)(2,1)} %bitcast.25), calls=%async_computation.4 | async-start | bytes 393216 | tf_op jit(solution)/shard_map/all_to_all | solution.py:150
  88.5 7.9 %all-to-all-done.4 = bf16[16,16,320]{2,1,0:T(8,128)(2,1)S(1)} async-done(((bf16[16,16,320]{2,1,0:T(8,128)(2,1)}), bf16[16,16,320]{2,1,0:T(8,128)(2,1)S(1)}, u32[]{:S(2)}, u32[]{:S(2)}) %all-to-all-start.4) | async-done | bytes 163872 | tf_op jit(solution)/shard_map/all_to_all | solution.py:150
  98.2 1.1 fusion.9
  99.3 1.3 fusion.14
  100.6 7.6 %multiply_add_fusion = f32[4,32,64,128]{3,2,1,0:T(8,128)S(1)} fusion(f32[4,32,64,128]{3,2,1,0:T(8,128)S(1)} %copy-done.2, f32[4,4,32,128]{3,1,2,0:T(4,128)S(1)} %bitcast.104, f32[4,32]{1,0:T(4,128)S(1)} %exp.62, f32[4,4,32,64]{3,2,1,0:T(8,128)S(1)} %reshape.159, f32[4,4,32]{1,2,0:T(8,128)S(1)} %copy.187), kind=kOutput, calls=%fused_computation.3 | convolution fusion | flops 52461568 | bytes 8784384 | tf_op jit(solution)/shard_map/vmap(sh,shp,shn->hpn)/dot_general | solution.py:60
  108.2 2.0 copy-done.1
  110.2 6.8 %fusion.67 = f32[4,32,64,4]{2,3,1,0:T(4,128)S(1)} fusion(f32[4,32,64,128]{3,2,1,0:T(8,128)S(1)} %multiply_add_fusion, f32[4,4,32,128]{3,1,2,0:T(4,128)S(1)} %bitcast.103), kind=kOutput, calls=%fused_computation.121 | convolution fusion | flops 50331648 | bytes 4587520 | tf_op jit(solution)/shard_map/vmap(thn,hpn->thp)/dot_general | solution.py:85
  117.9 103.2 %all-gather.5.cloned.1.call-done = bf16[2048,2048]{1,0:T(8,128)(2,1)} async-done(((bf16[2048,128]{1,0:T(8,128)(2,1)}), bf16[2048,2048]{1,0:T(8,128)(2,1)}) %all-gather.5.cloned.1.call-update) | async-done | bytes 8388624 | tf_op jit(solution)/shard_map/all_gather | solution.py:187
  221.0 5.2 %convolution_convert_fusion = bf16[16,2048]{1,0:T(8,128)(2,1)} fusion(bf16[2048,2048]{1,0:T(8,128)(2,1)} %all-gather.5.cloned.1.call-done, f32[16,2048]{1,0:T(8,128)S(1)} %bitcast.105, f32[16,2048]{1,0:T(8,128)S(1)} %reshape.169, f32[16,2,8,128]{3,2,1,0:T(8,128)S(1)} %get-tuple-element.40, f32[2048]{0:T(1024)S(1)} %copy-done.11), kind=kOutput, calls=%fused_computation.4 | convolution fusion | flops 134512640 | bytes 8855552 | tf_op jit(solution)/shard_map/dot_general | solution.py:185
  228.3 3.9 %reduce-scatter.2.cloned.1.call-done = bf16[16,1024]{1,0:T(8,128)(2,1)} async-done(((bf16[16,2048]{1,0:T(8,128)(2,1)}), bf16[16,1024]{1,0:T(8,128)(2,1)}) %reduce-scatter.2.cloned.1.call-update) | async-done | bytes 32784 | tf_op jit(solution)/shard_map/reduce_scatter | solution.py:190
  232.2 1.4 reshape.170
  (107 shorter events, 13.2 us)
Async XLA Ops:
  7.2 38.9 %copy-start = (bf16[2048,64]{0,1:T(8,128)(2,1)S(1)}, bf16[2048,64]{0,1:T(8,128)(2,1)}, u32[]{:S(2)}) copy-start(bf16[2048,64]{0,1:T(8,128)(2,1)} %param.27) | copy-start | bytes 786436
  7.2 37.8 %copy-start.7 = (bf16[128,2048]{1,0:T(8,128)(2,1)S(1)}, bf16[128,2048]{1,0:T(8,128)(2,1)}, u32[]{:S(2)}) copy-start(bf16[128,2048]{1,0:T(8,128)(2,1)} %param.24) | copy-start | bytes 1572868
  7.2 38.8 %copy-start.17 = (s32[4]{0:T(128)S(1)}, s32[4]{0:T(128)}, u32[]{:S(2)}) copy-start(s32[4]{0:T(128)} %param.41) | copy-start | bytes 52
  7.2 38.8 %copy-start.16 = (f32[32]{0:T(128)S(1)}, f32[32]{0:T(128)}, u32[]{:S(2)}) copy-start(f32[32]{0:T(128)} %param.32) | copy-start | bytes 388
  7.2 39.0 %copy-start.14 = (f32[32]{0:T(128)S(1)}, f32[32]{0:T(128)}, u32[]{:S(2)}) copy-start(f32[32]{0:T(128)} %param.31) | copy-start | bytes 388
  7.2 39.0 %copy-start.10 = (bf16[4,4,32]{2,1,0:T(4,128)(2,1)S(1)}, bf16[4,4,32]{2,1,0:T(4,128)(2,1)}, u32[]{:S(2)}) copy-start(bf16[4,4,32]{2,1,0:T(4,128)(2,1)} %param.40) | copy-start | bytes 3076
  7.2 56.5 %copy-start.3 = (bf16[4,7,2048]{2,0,1:T(4,128)(2,1)S(1)}, bf16[4,7,2048]{2,0,1:T(4,128)(2,1)}, u32[]{:S(2)}) copy-start(bf16[4,7,2048]{2,0,1:T(4,128)(2,1)} %param.37) | copy-start | bytes 344068
  7.2 57.4 %copy-start.4 = (bf16[4,7,512]{2,0,1:T(4,128)(2,1)S(1)}, bf16[4,7,512]{2,0,1:T(4,128)(2,1)}, u32[]{:S(2)}) copy-start(bf16[4,7,512]{2,0,1:T(4,128)(2,1)} %param.38) | copy-start | bytes 86020
  7.3 58.3 %copy-start.5 = (bf16[4,7,512]{2,0,1:T(4,128)(2,1)S(1)}, bf16[4,7,512]{2,0,1:T(4,128)(2,1)}, u32[]{:S(2)}) copy-start(bf16[4,7,512]{2,0,1:T(4,128)(2,1)} %param.39) | copy-start | bytes 86020
  7.3 59.0 %copy-start.12 = (f32[4,512]{1,0:T(4,128)S(1)}, f32[4,512]{1,0:T(4,128)}, u32[]{:S(2)}) copy-start(f32[4,512]{1,0:T(4,128)} %param.29) | copy-start | bytes 24580
  7.3 59.1 %copy-start.8 = (f32[4,2048]{1,0:T(4,128)S(1)}, f32[4,2048]{1,0:T(4,128)}, u32[]{:S(2)}) copy-start(f32[4,2048]{1,0:T(4,128)} %param.28) | copy-start | bytes 98308
  7.3 73.1 %all-gather.3.cloned.1.call-start = ((), (), s32[]{:S(2)}) async-start(), calls=%async_computation.6 | async-start | bytes 1114112 | tf_op jit(solution)/shard_map/all_gather | solution.py:148
  11.3 34.8 %copy-start.6 = (bf16[16,2048]{1,0:T(8,128)(2,1)S(1)}, bf16[16,2048]{1,0:T(8,128)(2,1)}, u32[]{:S(2)}) copy-start(bf16[16,2048]{1,0:T(8,128)(2,1)} %reshape.162) | copy-start | bytes 196612
  11.3 209.8 %all-gather.5.cloned.1.call-start = ((), (), s32[]{:S(2)}) async-start(), calls=%async_computation.7 | async-start | bytes 8912896 | tf_op jit(solution)/shard_map/all_gather | solution.py:187
  13.7 16.4 %all-to-all-start.2 = ((bf16[128,16,32]{0,2,1:T(8,128)(2,1)}), bf16[128,16,32]{0,2,1:T(8,128)(2,1)S(1)}, u32[]{:S(2)}, u32[]{:S(2)}) async-start(bf16[128,16,32]{0,2,1:T(8,128)(2,1)} %bitcast.19), calls=%async_computation.2 | async-start | bytes 262144 | tf_op jit(solution)/shard_map/all_to_all | solution.py:142
  30.1 11.3 %all-to-all-start.3 = ((bf16[128,16,32]{0,2,1:T(8,128)(2,1)}), bf16[128,16,32]{0,2,1:T(8,128)(2,1)S(1)}, u32[]{:S(2)}, u32[]{:S(2)}) async-start(bf16[128,16,32]{0,2,1:T(8,128)(2,1)} %bitcast.22), calls=%async_computation.3 | async-start | bytes 262144 | tf_op jit(solution)/shard_map/all_to_all | solution.py:143
  41.4 18.3 %all-to-all-start = ((bf16[128,16,128]{0,2,1:T(8,128)(2,1)}), bf16[128,16,128]{0,2,1:T(8,128)(2,1)S(1)}, u32[]{:S(2)}, u32[]{:S(2)}) async-start(bf16[128,16,128]{0,2,1:T(8,128)(2,1)} %bitcast.13), calls=%async_computation | async-start | bytes 1048576 | tf_op jit(solution)/shard_map/all_to_all | solution.py:140
  46.2 36.4 %copy-start.9 = (bf16[16,32]{1,0:T(8,128)(2,1)}, bf16[16,32]{1,0:T(8,128)(2,1)S(1)}, u32[]{:S(2)}) copy-start(bf16[16,32]{1,0:T(8,128)(2,1)S(1)} %convolution_convert_fusion.1) | copy-start | bytes 3076
  59.6 20.4 %all-to-all-start.1 = ((bf16[128,16,128]{0,2,1:T(8,128)(2,1)}), bf16[128,16,128]{0,2,1:T(8,128)(2,1)S(1)}, u32[]{:S(2)}, u32[]{:S(2)}) async-start(bf16[128,16,128]{0,2,1:T(8,128)(2,1)} %bitcast.16), calls=%async_computation.1 | async-start | bytes 1048576 | tf_op jit(solution)/shard_map/all_to_all | solution.py:141
  80.0 8.5 %copy-start.13 = (f32[4,512]{1,0:T(4,128)S(1)}, f32[4,512]{1,0:T(4,128)}, u32[]{:S(2)}) copy-start(f32[4,512]{1,0:T(4,128)} %param.30) | copy-start | bytes 24580
  83.5 13.0 %all-to-all-start.4 = ((bf16[16,16,320]{2,1,0:T(8,128)(2,1)}), bf16[16,16,320]{2,1,0:T(8,128)(2,1)S(1)}, u32[]{:S(2)}, u32[]{:S(2)}) async-start(bf16[16,16,320]{2,1,0:T(8,128)(2,1)} %bitcast.25), calls=%async_computation.4 | async-start | bytes 393216 | tf_op jit(solution)/shard_map/all_to_all | solution.py:150
  88.3 143.9 %reduce-scatter.2.cloned.1.call-start = ((), (), s32[]{:S(2)}) async-start(), calls=%async_computation.8 | async-start | bytes 98304 | tf_op jit(solution)/shard_map/reduce_scatter | solution.py:190
  110.2 6.8 %copy-start.15 = (f32[32]{0:T(128)S(1)}, f32[32]{0:T(128)}, u32[]{:S(2)}) copy-start(f32[32]{0:T(128)} %param.33) | copy-start | bytes 388
  110.2 110.8 %copy-start.11 = (f32[2048]{0:T(1024)S(1)}, f32[2048]{0:T(1024)}, u32[]{:S(2)}) copy-start(f32[2048]{0:T(1024)} %param.34) | copy-start | bytes 24580
  (2 other events, 4.7 us)
Sparse Core Ops, SparseCore 0:
  11.4 63.3 all-gather.2
  77.5 143.4 all-gather.4
  226.4 5.7 reduce-scatter.1
where the time goes:
time: 241 us; the launch traced here: 240 us
  waiting for transfers between devices  154 us (64%)
  matrix products  24.4 us (10%)
  starting transfers between devices  24.3 us (10%)
  local copies, waits for them, and re-layouts  18.5 us (8%)
  between operations  14.2 us (6%)
    all_gather x1, waiting for transfers between devices, on_device(): lax.all_gather(out_weight, 'kv', axis=1, tiled=True)  103 us
    all_to_all x1, waiting for transfers between devices, on_device(): lax.all_to_all(gate_weight, 'kv', split_axis=1, concat_axis=0, tiled=True)  13.3 us
    all_to_all x1, waiting for transfers between devices, on_device(): lax.all_to_all(value_weight, 'kv', split_axis=1, concat_axis=0, tiled=True)  12.8 us
    unnamed x45, local copies, waits for them, and re-layouts  10.6 us
    all_to_all x1, starting transfers between devices, on_device(): lax.all_to_all(write_weight, 'kv', split_axis=1, concat_axis=0, tiled=True)  8.2 us
    all_to_all x1, waiting for transfers between devices, on_device(): lax.all_to_all(everyone, 'kv', split_axis=0, concat_axis=1, tiled=True)  7.89 us
    dot_general x1, matrix products, advance(): jnp.einsum('sh,shp,shn->hpn', weight_now, prev_x, prev_b, precision=highest)  7.61 us
    dot_general x1, matrix products, advance(): jnp.einsum('thn,hpn->thp', cur_c, root, precision=highest)  6.79 us
  transfers between devices with their start and end apart: 8, of which 7 were waited for; matrix products, arithmetic and copies ran while one was open for 15% of the time, Pallas kernels for 0%

commit v1 on v0

--- a/solution.py
+++ b/solution.py
@@ -6,6 +6,11 @@
 STATE_DIM = 128
 CONV_W = 4
 EPSILON = 1e-06
+
+
+def stack_and_merge(value, name, dim):
+    parts = lax.all_gather(value, name)
+    return jnp.concatenate(parts, axis=dim)
 
 
 def causal_conv(rows, kernel):
@@ -183,9 +188,7 @@
     )
     flat_y = normal_out.reshape(token_count, -1)
     partial_sum = jnp.dot(
-        flat_y,
-        lax.all_gather(out_weight, "kv", axis=1, tiled=True),
-        preferred_element_type=jnp.float32,
+        flat_y, stack_and_merge(out_weight, "kv", 1), preferred_element_type=jnp.float32
     )
     summed = lax.psum_scatter(
         partial_sum.astype(jnp.bfloat16), "tp", scatter_dimension=1, tiled=True

time: 241 us -> 227 us (0.942)
  waiting for transfers between devices: 154 us -> 126 us
  local copies, waits for them, and re-layouts: 18.5 us -> 30.5 us
    all_gather x1, waiting for transfers between devices: 103 us -> 71.4 us  [stack_and_merge(): parts = lax.all_gather(value, name)]
    reshape x0 -> x1, local copies, waits for them, and re-layouts: none -> 12 us  [stack_and_merge(): return jnp.concatenate(parts, axis=dim)]
    all_to_all x1, waiting for transfers between devices: 7.89 us -> 11.8 us  [on_device(): lax.all_to_all(everyone, 'kv', split_axis=0, concat_axis=1, tiled=True)]
  transfers between devices with their start and end apart: 8 -> 8, of which waited for: 7 -> 7; matrix products, arithmetic and copies ran while one was open for 15% -> 16% of each run, Pallas kernels for 0% -> 0%
where the time goes in v1:
time: 227 us; the launch traced here: 225 us
  waiting for transfers between devices  126 us (56%)
  local copies, waits for them, and re-layouts  30.5 us (13%)
  matrix products  25.5 us (11%)
  starting transfers between devices  24.3 us (11%)
  between operations  14.3 us (6%)
  other arithmetic  2.4 us (1%)
  blocking collectives  2.34 us (1%)
    all_gather x1, waiting for transfers between devices, stack_and_merge(): parts = lax.all_gather(value, name)  71.4 us
    all_to_all x1, waiting for transfers between devices, on_device(): lax.all_to_all(gate_weight, 'kv', split_axis=1, concat_axis=0, tiled=True)  13.3 us
    all_to_all x1, waiting for transfers between devices, on_device(): lax.all_to_all(value_weight, 'kv', split_axis=1, concat_axis=0, tiled=True)  12.8 us
    reshape x1, local copies, waits for them, and re-layouts, stack_and_merge(): return jnp.concatenate(parts, axis=dim)  12 us
    all_to_all x1, waiting for transfers between devices, on_device(): lax.all_to_all(everyone, 'kv', split_axis=0, concat_axis=1, tiled=True)  11.8 us
    unnamed x45, local copies, waits for them, and re-layouts  10.6 us
    all_to_all x1, starting transfers between devices, on_device(): lax.all_to_all(write_weight, 'kv', split_axis=1, concat_axis=0, tiled=True)  8.2 us
    dot_general x1, matrix products, advance(): jnp.einsum('sh,shp,shn->hpn', weight_now, prev_x, prev_b, precision=highest)  7.61 us
  transfers between devices with their start and end apart: 8, of which 7 were waited for; matrix products, arithmetic and copies ran while one was open for 16% of the time, Pallas kernels for 0%

profile of v1, /device:TPU:0, one launch (start us, length us, event | category | flops | bytes accessed | tf_op | source)
XLA Modules:
  0.0 225.4 jit_solution(8584618440573531595)
XLA Ops:
  7.3 2.3 %all_gather.12 = bf16[4,4,2048]{2,1,0:T(4,128)(2,1)S(1)} all-gather(bf16[4,4,1024]{2,1,0:T(4,128)(2,1)} %param.21), channel_id=1, replica_groups=mesh['kv'=16,'tp'=2] {'tp'}, dimensions={2}, use_global_device_ids=true | all-gather | bytes 98304 | tf_op jit(solution)/shard_map/all_gather | solution.py:131
  12.1 1.7 copy.199
  13.7 8.2 %all-to-all-start.2 = ((bf16[128,16,32]{0,2,1:T(8,128)(2,1)}), bf16[128,16,32]{0,2,1:T(8,128)(2,1)S(1)}, u32[]{:S(2)}, u32[]{:S(2)}) async-start(bf16[128,16,32]{0,2,1:T(8,128)(2,1)} %bitcast.19), calls=%async_computation.2 | async-start | bytes 262144 | tf_op jit(solution)/shard_map/all_to_all | solution.py:147
  21.9 1.7 copy.201
  23.6 6.5 %all-to-all-done.2 = bf16[128,16,32]{0,2,1:T(8,128)(2,1)S(1)} async-done(((bf16[128,16,32]{0,2,1:T(8,128)(2,1)}), bf16[128,16,32]{0,2,1:T(8,128)(2,1)S(1)}, u32[]{:S(2)}, u32[]{:S(2)}) %all-to-all-start.2) | async-done | bytes 131104 | tf_op jit(solution)/shard_map/all_to_all | solution.py:147
  30.1 3.5 %all-to-all-start.3 = ((bf16[128,16,32]{0,2,1:T(8,128)(2,1)}), bf16[128,16,32]{0,2,1:T(8,128)(2,1)S(1)}, u32[]{:S(2)}, u32[]{:S(2)}) async-start(bf16[128,16,32]{0,2,1:T(8,128)(2,1)} %bitcast.22), calls=%async_computation.3 | async-start | bytes 262144 | tf_op jit(solution)/shard_map/all_to_all | solution.py:148
  33.6 2.0 copy.195
  35.7 5.7 %all-to-all-done.3 = bf16[128,16,32]{0,2,1:T(8,128)(2,1)S(1)} async-done(((bf16[128,16,32]{0,2,1:T(8,128)(2,1)}), bf16[128,16,32]{0,2,1:T(8,128)(2,1)S(1)}, u32[]{:S(2)}, u32[]{:S(2)}) %all-to-all-start.3) | async-done | bytes 131104 | tf_op jit(solution)/shard_map/all_to_all | solution.py:148
  41.4 3.6 %all-to-all-start = ((bf16[128,16,128]{0,2,1:T(8,128)(2,1)}), bf16[128,16,128]{0,2,1:T(8,128)(2,1)S(1)}, u32[]{:S(2)}, u32[]{:S(2)}) async-start(bf16[128,16,128]{0,2,1:T(8,128)(2,1)} %bitcast.13), calls=%async_computation | async-start | bytes 1048576 | tf_op jit(solution)/shard_map/all_to_all | solution.py:145
  46.3 13.3 %all-to-all-done = bf16[128,16,128]{0,2,1:T(8,128)(2,1)S(1)} async-done(((bf16[128,16,128]{0,2,1:T(8,128)(2,1)}), bf16[128,16,128]{0,2,1:T(8,128)(2,1)S(1)}, u32[]{:S(2)}, u32[]{:S(2)}) %all-to-all-start) | async-done | bytes 524320 | tf_op jit(solution)/shard_map/all_to_all | solution.py:145
  59.7 3.9 %all-to-all-start.1 = ((bf16[128,16,128]{0,2,1:T(8,128)(2,1)}), bf16[128,16,128]{0,2,1:T(8,128)(2,1)S(1)}, u32[]{:S(2)}, u32[]{:S(2)}) async-start(bf16[128,16,128]{0,2,1:T(8,128)(2,1)} %bitcast.16), calls=%async_computation.1 | async-start | bytes 1048576 | tf_op jit(solution)/shard_map/all_to_all | solution.py:146
  67.3 12.8 %all-to-all-done.1 = bf16[128,16,128]{0,2,1:T(8,128)(2,1)S(1)} async-done(((bf16[128,16,128]{0,2,1:T(8,128)(2,1)}), bf16[128,16,128]{0,2,1:T(8,128)(2,1)S(1)}, u32[]{:S(2)}, u32[]{:S(2)}) %all-to-all-start.1) | async-done | bytes 524320 | tf_op jit(solution)/shard_map/all_to_all | solution.py:146
  80.4 2.3 %fusion.10 = bf16[256,320]{0,1:T(8,128)(2,1)S(1)} fusion(bf16[256,2048]{1,0:T(8,128)(2,1)} %all-gather.4.cloned.1.call-done, bf16[2048,32]{1,0:T(8,128)(2,1)S(1)} %bitcast.90, bf16[2048,32]{1,0:T(8,128)(2,1)S(1)} %bitcast.91, bf16[2048,128]{1,0:T(8,128)(2,1)S(1)} %bitcast.95, bf16[2048,128]{1,0:T(8,128)(2,1)S(1)} %bitcast.94), kind=kOutput, calls=%fused_computation.16 | convolution fusion | flops 340869120 | bytes 2523136 | tf_op jit(solution)/shard_map/dot_general | solution.py:152
  83.5 4.8 %all-to-all-start.4 = ((bf16[16,16,320]{2,1,0:T(8,128)(2,1)}), bf16[16,16,320]{2,1,0:T(8,128)(2,1)S(1)}, u32[]{:S(2)}, u32[]{:S(2)}) async-start(bf16[16,16,320]{2,1,0:T(8,128)(2,1)} %bitcast.25), calls=%async_computation.4 | async-start | bytes 393216 | tf_op jit(solution)/shard_map/all_to_all | solution.py:155
  88.6 11.8 %all-to-all-done.4 = bf16[16,16,320]{2,1,0:T(8,128)(2,1)S(1)} async-done(((bf16[16,16,320]{2,1,0:T(8,128)(2,1)}), bf16[16,16,320]{2,1,0:T(8,128)(2,1)S(1)}, u32[]{:S(2)}, u32[]{:S(2)}) %all-to-all-start.4) | async-done | bytes 163872 | tf_op jit(solution)/shard_map/all_to_all | solution.py:155
  103.3 1.3 fusion.14
  104.6 7.6 %multiply_add_fusion = f32[4,32,64,128]{3,2,1,0:T(8,128)S(1)} fusion(f32[4,32,64,128]{3,2,1,0:T(8,128)S(1)} %copy-done.2, f32[4,4,32,128]{3,1,2,0:T(4,128)S(1)} %bitcast.89, f32[4,32]{1,0:T(4,128)S(1)} %exp.69, f32[4,4,32,64]{3,2,1,0:T(8,128)S(1)} %reshape.212, f32[4,4,32]{1,2,0:T(8,128)S(1)} %copy.190), kind=kOutput, calls=%fused_computation.3 | convolution fusion | flops 52461568 | bytes 8784384 | tf_op jit(solution)/shard_map/vmap(sh,shp,shn->hpn)/dot_general | solution.py:65
  112.2 2.0 copy-done.1
  114.2 6.8 %fusion.57 = f32[4,32,64,4]{2,3,1,0:T(4,128)S(1)} fusion(f32[4,32,64,128]{3,2,1,0:T(8,128)S(1)} %multiply_add_fusion, f32[4,4,32,128]{3,1,2,0:T(4,128)S(1)} %bitcast.88), kind=kOutput, calls=%fused_computation.112 | convolution fusion | flops 50331648 | bytes 4587520 | tf_op jit(solution)/shard_map/vmap(thn,hpn->thp)/dot_general | solution.py:90
  121.9 71.4 %all-gather.6.cloned.1.call-done = bf16[32768,128]{1,0:T(8,128)(2,1)} async-done(((bf16[2048,128]{1,0:T(8,128)(2,1)}), bf16[32768,128]{1,0:T(8,128)(2,1)}) %all-gather.6.cloned.1.call-update) | async-done | bytes 8388624 | tf_op jit(solution)/shard_map/all_gather | solution.py:12
  193.3 12.0 %copy.225 = bf16[2048,16,128]{0,2,1:T(8,128)(2,1)} copy(bf16[2048,16,128]{2,0,1:T(8,128)(2,1)} %bitcast.82) | data formatting | bytes 16777216 | tf_op jit(solution)/shard_map/reshape | solution.py:13
  205.3 6.3 %convolution_convert_fusion = bf16[16,2048]{1,0:T(8,128)(2,1)} fusion(bf16[16,2048]{1,0:T(8,128)(2,1)S(1)} %bitcast.96, bf16[2048,2048]{0,1:T(8,128)(2,1)} %bitcast.81), kind=kOutput, calls=%fused_computation.4 | convolution fusion | flops 134250496 | bytes 8519680 | tf_op jit(solution)/shard_map/dot_general | solution.py:190
  213.6 3.9 %reduce-scatter.2.cloned.1.call-done = bf16[16,1024]{1,0:T(8,128)(2,1)} async-done(((bf16[16,2048]{1,0:T(8,128)(2,1)}), bf16[16,1024]{1,0:T(8,128)(2,1)}) %reduce-scatter.2.cloned.1.call-update) | async-done | bytes 32784 | tf_op jit(solution)/shard_map/reduce_scatter | solution.py:193
  217.5 1.4 reshape.225
  (110 shorter events, 14.4 us)
Async XLA Ops:
  7.2 38.9 %copy-start = (bf16[2048,64]{0,1:T(8,128)(2,1)S(1)}, bf16[2048,64]{0,1:T(8,128)(2,1)}, u32[]{:S(2)}) copy-start(bf16[2048,64]{0,1:T(8,128)(2,1)} %param.27) | copy-start | bytes 786436
  7.2 37.8 %copy-start.7 = (bf16[128,2048]{1,0:T(8,128)(2,1)S(1)}, bf16[128,2048]{1,0:T(8,128)(2,1)}, u32[]{:S(2)}) copy-start(bf16[128,2048]{1,0:T(8,128)(2,1)} %param.24) | copy-start | bytes 1572868
  7.2 38.8 %copy-start.17 = (s32[4]{0:T(128)S(1)}, s32[4]{0:T(128)}, u32[]{:S(2)}) copy-start(s32[4]{0:T(128)} %param.41) | copy-start | bytes 52
  7.2 38.8 %copy-start.16 = (f32[32]{0:T(128)S(1)}, f32[32]{0:T(128)}, u32[]{:S(2)}) copy-start(f32[32]{0:T(128)} %param.32) | copy-start | bytes 388
  7.2 39.0 %copy-start.10 = (bf16[4,4,32]{2,1,0:T(4,128)(2,1)S(1)}, bf16[4,4,32]{2,1,0:T(4,128)(2,1)}, u32[]{:S(2)}) copy-start(bf16[4,4,32]{2,1,0:T(4,128)(2,1)} %param.40) | copy-start | bytes 3076
  7.2 39.0 %copy-start.14 = (f32[32]{0:T(128)S(1)}, f32[32]{0:T(128)}, u32[]{:S(2)}) copy-start(f32[32]{0:T(128)} %param.31) | copy-start | bytes 388
  7.2 56.5 %copy-start.11 = (f32[2048]{0:T(1024)S(1)}, f32[2048]{0:T(1024)}, u32[]{:S(2)}) copy-start(f32[2048]{0:T(1024)} %param.34) | copy-start | bytes 24580
  7.2 56.5 %copy-start.4 = (bf16[4,7,512]{2,0,1:T(4,128)(2,1)S(1)}, bf16[4,7,512]{2,0,1:T(4,128)(2,1)}, u32[]{:S(2)}) copy-start(bf16[4,7,512]{2,0,1:T(4,128)(2,1)} %param.38) | copy-start | bytes 86020
  7.3 57.2 %copy-start.5 = (bf16[4,7,512]{2,0,1:T(4,128)(2,1)S(1)}, bf16[4,7,512]{2,0,1:T(4,128)(2,1)}, u32[]{:S(2)}) copy-start(bf16[4,7,512]{2,0,1:T(4,128)(2,1)} %param.39) | copy-start | bytes 86020
  7.3 57.9 %copy-start.3 = (bf16[4,7,2048]{2,0,1:T(4,128)(2,1)S(1)}, bf16[4,7,2048]{2,0,1:T(4,128)(2,1)}, u32[]{:S(2)}) copy-start(bf16[4,7,2048]{2,0,1:T(4,128)(2,1)} %param.37) | copy-start | bytes 344068
  7.3 59.1 %copy-start.12 = (f32[4,512]{1,0:T(4,128)S(1)}, f32[4,512]{1,0:T(4,128)}, u32[]{:S(2)}) copy-start(f32[4,512]{1,0:T(4,128)} %param.29) | copy-start | bytes 24580
  7.3 59.1 %copy-start.8 = (f32[4,2048]{1,0:T(4,128)S(1)}, f32[4,2048]{1,0:T(4,128)}, u32[]{:S(2)}) copy-start(f32[4,2048]{1,0:T(4,128)} %param.28) | copy-start | bytes 98308
  7.3 73.1 %all-gather.4.cloned.1.call-start = ((), (), s32[]{:S(2)}) async-start(), calls=%async_computation.6 | async-start | bytes 1114112 | tf_op jit(solution)/shard_map/all_gather | solution.py:153
  11.3 34.8 %copy-start.6 = (bf16[16,2048]{1,0:T(8,128)(2,1)S(1)}, bf16[16,2048]{1,0:T(8,128)(2,1)}, u32[]{:S(2)}) copy-start(bf16[16,2048]{1,0:T(8,128)(2,1)} %reshape.215) | copy-start | bytes 196612
  11.3 182.0 %all-gather.6.cloned.1.call-start = ((), (), s32[]{:S(2)}) async-start(), calls=%async_computation.8 | async-start | bytes 8912896 | tf_op jit(solution)/shard_map/all_gather | solution.py:12
  13.7 16.4 %all-to-all-start.2 = ((bf16[128,16,32]{0,2,1:T(8,128)(2,1)}), bf16[128,16,32]{0,2,1:T(8,128)(2,1)S(1)}, u32[]{:S(2)}, u32[]{:S(2)}) async-start(bf16[128,16,32]{0,2,1:T(8,128)(2,1)} %bitcast.19), calls=%async_computation.2 | async-start | bytes 262144 | tf_op jit(solution)/shard_map/all_to_all | solution.py:147
  30.1 11.3 %all-to-all-start.3 = ((bf16[128,16,32]{0,2,1:T(8,128)(2,1)}), bf16[128,16,32]{0,2,1:T(8,128)(2,1)S(1)}, u32[]{:S(2)}, u32[]{:S(2)}) async-start(bf16[128,16,32]{0,2,1:T(8,128)(2,1)} %bitcast.22), calls=%async_computation.3 | async-start | bytes 262144 | tf_op jit(solution)/shard_map/all_to_all | solution.py:148
  41.4 18.3 %all-to-all-start = ((bf16[128,16,128]{0,2,1:T(8,128)(2,1)}), bf16[128,16,128]{0,2,1:T(8,128)(2,1)S(1)}, u32[]{:S(2)}, u32[]{:S(2)}) async-start(bf16[128,16,128]{0,2,1:T(8,128)(2,1)} %bitcast.13), calls=%async_computation | async-start | bytes 1048576 | tf_op jit(solution)/shard_map/all_to_all | solution.py:145
  46.2 36.4 %copy-start.9 = (bf16[16,32]{1,0:T(8,128)(2,1)}, bf16[16,32]{1,0:T(8,128)(2,1)S(1)}, u32[]{:S(2)}) copy-start(bf16[16,32]{1,0:T(8,128)(2,1)S(1)} %convolution_convert_fusion.1) | copy-start | bytes 3076
  59.7 20.4 %all-to-all-start.1 = ((bf16[128,16,128]{0,2,1:T(8,128)(2,1)}), bf16[128,16,128]{0,2,1:T(8,128)(2,1)S(1)}, u32[]{:S(2)}, u32[]{:S(2)}) async-start(bf16[128,16,128]{0,2,1:T(8,128)(2,1)} %bitcast.16), calls=%async_computation.1 | async-start | bytes 1048576 | tf_op jit(solution)/shard_map/all_to_all | solution.py:146
  80.0 8.5 %copy-start.13 = (f32[4,512]{1,0:T(4,128)S(1)}, f32[4,512]{1,0:T(4,128)}, u32[]{:S(2)}) copy-start(f32[4,512]{1,0:T(4,128)} %param.30) | copy-start | bytes 24580
  83.5 16.9 %all-to-all-start.4 = ((bf16[16,16,320]{2,1,0:T(8,128)(2,1)}), bf16[16,16,320]{2,1,0:T(8,128)(2,1)S(1)}, u32[]{:S(2)}, u32[]{:S(2)}) async-start(bf16[16,16,320]{2,1,0:T(8,128)(2,1)} %bitcast.25), calls=%async_computation.4 | async-start | bytes 393216 | tf_op jit(solution)/shard_map/all_to_all | solution.py:155
  88.3 129.2 %reduce-scatter.2.cloned.1.call-start = ((), (), s32[]{:S(2)}) async-start(), calls=%async_computation.7 | async-start | bytes 98304 | tf_op jit(solution)/shard_map/reduce_scatter | solution.py:193
  114.2 6.8 %copy-start.15 = (f32[32]{0:T(128)S(1)}, f32[32]{0:T(128)}, u32[]{:S(2)}) copy-start(f32[32]{0:T(128)} %param.33) | copy-start | bytes 388
  (2 other events, 4.7 us)
Sparse Core Ops, SparseCore 0:
  11.4 63.3 all-gather.3
  77.6 115.6 all-gather.5
  211.7 5.7 reduce-scatter.1
